TPU v7x, 32 devices: a whole 2x2x4 slice. The times are simulated.
32 devices in a mesh: sp: 16 (over z, y, x), tp: 2 (over core).
Axes of the slice: x: 2, y: 2, z: 4, core: 2. Of those that a mesh axis runs over, the one named last changes fastest.
Arguments:
- queries: bfloat16 [8192, 8, 128], P('sp', 'tp'), may hold values from -60 to 60
- keys: bfloat16 [8192, 8, 128], P('sp', 'tp'), may hold values from -40 to 40
- values: bfloat16 [8192, 8, 128], P('sp', 'tp'), may hold values from -6 to 6
- w_out: bfloat16 [1024, 2048], P(None, 'tp'), may hold values from -0.1875 to 0.1875
Outputs:
- mixed: bfloat16 [8192, 2048], P('sp', 'tp')
All inputs are finite; a program needn't handle non-finite values.
Results may differ from a plain program's by a relative error of at most 0.0051.
Values may be sent and summed in bfloat16 or wider, within the bound.
A program may use at most 64 MiB of HBM per device.

v0:
```python
import math

import jax
import jax.numpy as jnp
from jax import lax
from jax.sharding import PartitionSpec as P

W1 = 128
WINDOW_TWO = 512
DILATION_TWO = 4
WINDOW_THREE = 2048
DILATION_THREE = 16


def from_behind(block, axis, distance):
    devices = range(lax.axis_size(axis))
    route = [(i - distance, i) for i in devices if i - distance in devices]
    return lax.ppermute(block, axis, route)


def branch_attend(queries, key_holder, value_holder, leading_total, leading_row, window, dilation):
    tok_rows, head_local, head_dim = queries.shape
    band_rows = window // dilation
    query_rows = tok_rows // dilation
    lead_rows = leading_total // dilation
    query_res = queries.reshape(query_rows, dilation, head_local, head_dim)
    key_res = key_holder.reshape(-1, dilation, head_local, head_dim)[
        lead_rows - band_rows : lead_rows + query_rows
    ]
    value_res = value_holder.reshape(-1, dilation, head_local, head_dim)[
        lead_rows - band_rows : lead_rows + query_rows
    ]
    scores = jnp.einsum(
        "qrhd,krhd->rhqk", query_res, key_res, preferred_element_type=jnp.float32
    ) / math.sqrt(head_dim)
    query_idx = jnp.arange(query_rows, dtype=jnp.int32)[:, None]
    key_idx = jnp.arange(query_rows + band_rows, dtype=jnp.int32)[None, :]
    distance = query_idx + band_rows - key_idx
    allowed = (
        (distance >= 0)
        & (distance <= band_rows)
        & (leading_row // dilation + key_idx - band_rows >= 0)
    )
    scores = jnp.where(allowed[None, None], scores, -jnp.inf)
    row_max = jnp.max(scores, axis=-1, keepdims=True)
    numerators = jnp.exp(scores - row_max)
    row_sum = jnp.sum(numerators, axis=-1, keepdims=True)
    weighted = jnp.einsum(
        "rhqk,krhd->qrhd",
        numerators.astype(jnp.bfloat16),
        value_res,
        preferred_element_type=jnp.float32,
    )
    branch_out = (weighted / jnp.transpose(row_sum, (2, 0, 1, 3))).reshape(
        tok_rows, head_local, head_dim
    )
    log_total = jnp.transpose((row_max + jnp.log(row_sum))[..., 0], (2, 0, 1)).reshape(
        tok_rows, head_local
    )
    return (branch_out, log_total)


def local(queries, keys, values, w_out):
    tok_rows, head_local, head_dim = queries.shape
    reach_pieces = WINDOW_THREE // tok_rows
    key_holder = keys
    value_holder = values
    covered = 0
    while covered < reach_pieces:
        distance = covered + 1
        amount = min(distance, reach_pieces - covered)
        moved_keys, moved_values = from_behind(
            (key_holder[-amount * tok_rows :], value_holder[-amount * tok_rows :]), "sp", distance
        )
        key_holder = jnp.concatenate([moved_keys, key_holder], axis=0)
        value_holder = jnp.concatenate([moved_values, value_holder], axis=0)
        covered = covered + amount
    leading_row = lax.axis_index("sp") * tok_rows
    leading_total = reach_pieces * tok_rows
    first_out, first_total = branch_attend(
        queries, key_holder, value_holder, leading_total, leading_row, W1, 1
    )
    second_output, second_branch_total = branch_attend(
        queries, key_holder, value_holder, leading_total, leading_row, WINDOW_TWO, DILATION_TWO
    )
    third_output, third_branch_total = branch_attend(
        queries, key_holder, value_holder, leading_total, leading_row, WINDOW_THREE, DILATION_THREE
    )
    weights = jax.nn.softmax(
        jnp.stack([first_total, second_branch_total, third_branch_total]), axis=0
    )
    combined = jnp.sum(
        weights[..., None] * jnp.stack([first_out, second_output, third_output]), axis=0
    )
    attended = combined.reshape(tok_rows, head_local * head_dim).astype(jnp.bfloat16)
    projected = jnp.dot(
        lax.all_gather(attended, "tp", axis=1, tiled=True),
        w_out,
        preferred_element_type=jnp.float32,
    )
    return projected.astype(jnp.bfloat16)


def solution(mesh):
    in_specs = (P("sp", "tp", None), P("sp", "tp", None), P("sp", "tp", None), P(None, "tp"))
    out_specs = P("sp", "tp")
    return jax.shard_map(local, mesh=mesh, in_specs=in_specs, out_specs=out_specs, check_vma=False)
```

profile of v0, /device:TPU:0, one launch (start us, length us, event | category | flops | bytes accessed | tf_op | source)
XLA Modules:
  0.0 158.3 jit_solution(2526331905830689763)
XLA Ops:
  7.8 5.8 %collective-permute-start.1 = (bf16[512,4,128]{2,0,1:T(8,128)(2,1)S(1)}, bf16[512,4,128]{2,0,1:T(8,128)(2,1)}, u32[]{:S(2)}, u32[]{:S(2)}) collective-permute-start(bf16[512,4,128]{2,0,1:T(8,128)(2,1)S(1)} %copy.55), channel_id=1, source_target_pairs={{0,8},{2,10},{4,12},{6,14},{8,16},{10,18},{12,20},{14,22},{16,24},... | collective-permute-start | bytes 1572872 | tf_op jit(solution)/shard_map/ppermute | solution.py:18
  13.6 4.2 %collective-permute-start = (bf16[512,4,128]{2,0,1:T(8,128)(2,1)S(1)}, bf16[512,4,128]{2,0,1:T(8,128)(2,1)}, u32[]{:S(2)}, u32[]{:S(2)}) collective-permute-start(bf16[512,4,128]{2,0,1:T(8,128)(2,1)S(1)} %copy.55), channel_id=1, source_target_pairs={{0,2},{2,4},{4,6},{6,8},{8,10},{10,12},{12,14},{14,16},{16,18},{18... | collective-permute-start | bytes 1572872 | tf_op jit(solution)/shard_map/ppermute | solution.py:18
  19.1 2.7 %collective-permute-start.4 = (bf16[512,4,128]{0,2,1:T(8,128)(2,1)S(1)}, bf16[512,4,128]{0,2,1:T(8,128)(2,1)}, u32[]{:S(2)}, u32[]{:S(2)}) collective-permute-start(bf16[512,4,128]{0,2,1:T(8,128)(2,1)S(1)} %copy.68), channel_id=1, source_target_pairs={{0,8},{2,10},{4,12},{6,14},{8,16},{10,18},{12,20},{14,22},{16,24},... | collective-permute-start | bytes 1572872 | tf_op jit(solution)/shard_map/ppermute | solution.py:18
  21.8 4.2 %collective-permute-start.3 = (bf16[512,4,128]{0,2,1:T(8,128)(2,1)S(1)}, bf16[512,4,128]{0,2,1:T(8,128)(2,1)}, u32[]{:S(2)}, u32[]{:S(2)}) collective-permute-start(bf16[512,4,128]{0,2,1:T(8,128)(2,1)S(1)} %copy.68), channel_id=1, source_target_pairs={{0,2},{2,4},{4,6},{6,8},{8,10},{10,12},{12,14},{14,16},{16,18},{18... | collective-permute-start | bytes 1572872 | tf_op jit(solution)/shard_map/ppermute | solution.py:18
  27.3 11.8 %collective-permute-done.3 = bf16[512,4,128]{0,2,1:T(8,128)(2,1)} collective-permute-done((bf16[512,4,128]{0,2,1:T(8,128)(2,1)S(1)}, bf16[512,4,128]{0,2,1:T(8,128)(2,1)}, u32[]{:S(2)}, u32[]{:S(2)}) %collective-permute-start.3) | collective-permute-done | bytes 524320 | tf_op jit(solution)/shard_map/ppermute | solution.py:18
  39.1 2.2 %pad_maximum_fusion.2 = bf16[1024,4,128]{0,2,1:T(8,128)(2,1)} fusion(bf16[512,4,128]{0,2,1:T(8,128)(2,1)S(1)} %copy.68, bf16[512,4,128]{0,2,1:T(8,128)(2,1)} %collective-permute-done.3), kind=kLoop, calls=%fused_computation.38 | loop fusion | flops 2097152 | bytes 2097152 | tf_op jit(solution)/shard_map/concatenate | solution.py:76
  41.3 2.3 %copy.71 = bf16[1024,4,128]{2,0,1:T(8,128)(2,1)} copy(bf16[1024,4,128]{0,2,1:T(8,128)(2,1)} %pad_maximum_fusion.2) | data formatting | bytes 2097152 | tf_op jit(solution)/shard_map/concatenate | solution.py:76
  43.5 6.5 %collective-permute-start.5 = (bf16[1024,4,128]{0,2,1:T(8,128)(2,1)}, bf16[1024,4,128]{0,2,1:T(8,128)(2,1)}, u32[]{:S(2)}, u32[]{:S(2)}) collective-permute-start(bf16[1024,4,128]{0,2,1:T(8,128)(2,1)} %pad_maximum_fusion.2), channel_id=1, source_target_pairs={{0,4},{2,6},{4,8},{6,10},{8,12},{10,14},{12,16},{14,18},{16,20},{1... | collective-permute-start | bytes 3145736 | tf_op jit(solution)/shard_map/ppermute | solution.py:18
  50.0 1.9 %constant_dynamic-update-slice_fusion.1 = bf16[1024,4,128]{2,0,1:T(8,128)(2,1)} fusion(bf16[512,4,128]{2,0,1:T(8,128)(2,1)} %collective-permute-done), kind=kLoop, calls=%fused_computation.70 | loop fusion | bytes 1048576
  51.9 2.0 %constant_dynamic-update-slice_fusion = bf16[1024,4,128]{2,0,1:T(8,128)(2,1)} fusion(bf16[1024,4,128]{2,0,1:T(8,128)(2,1)} %constant_dynamic-update-slice_fusion.1, bf16[512,4,128]{2,1,0:T(4,128)(2,1)} %param.5), kind=kLoop, calls=%fused_computation.69 | loop fusion | bytes 1048576 | tf_op jit(solution)/shard_map/concatenate | solution.py:75
  53.9 22.8 %collective-permute-start.2 = (bf16[1024,4,128]{2,0,1:T(8,128)(2,1)}, bf16[1024,4,128]{2,0,1:T(8,128)(2,1)}, u32[]{:S(2)}, u32[]{:S(2)}) collective-permute-start(bf16[1024,4,128]{2,0,1:T(8,128)(2,1)} %constant_dynamic-update-slice_fusion), channel_id=1, source_target_pairs={{0,4},{2,6},{4,8},{6,10},{8,12},{10,14},{12,16},{14,18},{16,20},{1... | collective-permute-start | bytes 3145736 | tf_op jit(solution)/shard_map/ppermute | solution.py:18
  80.5 2.6 %fusion.26 = f32[128,4,4,128]{3,0,2,1:T(8,128)S(1)} fusion(f32[4,4,128,256]{2,3,1,0:T(8,128)} %copy-done.3, bf16[256,4,4,128]{3,1,0,2:T(4,128)(2,1)} %bitcast.87, f32[4,4,128]{2,1,0:T(4,128)S(1)} %get-tuple-element.7, f32[128,4,4]{0,2,1:T(4,128)S(1)} %bitcast.90), kind=kOutput, calls=%fused_computation.30 | convolution fusion | flops 135528448 | bytes 4210688 | tf_op jit(solution)/shard_map/rhqk,krhd->qrhd/dot_general | solution.py:48
  84.8 2.5 %copy.80 = f32[1,512,4,128]{1,3,2,0:T(8,128)} copy(f32[1,512,4,128]{3,1,2,0:T(8,128)} %bitcast.82) | data formatting | bytes 2097152 | tf_op jit(solution)/shard_map/stack;reshape | solution.py:93
  87.4 2.4 %fusion.2 = (f32[4,512]{1,0:T(4,128)S(1)}, f32[4,640,512]{2,1,0:T(8,128)S(1)}) fusion(pred[512,640]{0,1:T(8,128)(4,1)} %fusion.30, bf16[512,4,128]{2,1,0:T(4,128)(2,1)} %param.4, bf16[1024,4,128]{2,0,1:T(8,128)(2,1)} %constant_dynamic-update-slice_fusion), kind=kOutput, calls=%fused_computation.4 | convolution fusion | flops 339474432 | bytes 6758400 | tf_op jit(solution)/shard_map/qrhd,krhd->rhqk/dot_general | solution.py:33
  90.9 3.5 %divide_bitcast_fusion = f32[1,512,4,128]{1,3,2,0:T(8,128)} fusion(f32[4,640,512]{2,1,0:T(8,128)S(1)} %get-tuple-element.10, f32[4,512]{1,0:T(4,128)S(1)} %get-tuple-element.9, pred[512,640]{0,1:T(8,128)(4,1)S(1)} %copy-done.4, bf16[512,4,128]{0,2,1:T(8,128)(2,1)} %collective-permute-done.3, bf16[512,4,128]{0,2,1:T(8,128)(2,1)S(1)} %copy.68, ...), kind=kOutput, calls=%fused_computation.42 | convolution fusion | flops 342360064 | bytes 7684096 | tf_op jit(solution)/shard_map/rhqk,krhd->qrhd/dot_general | solution.py:48
  94.4 2.9 %collective-permute-done.2 = bf16[1024,4,128]{2,0,1:T(8,128)(2,1)} collective-permute-done((bf16[1024,4,128]{2,0,1:T(8,128)(2,1)}, bf16[1024,4,128]{2,0,1:T(8,128)(2,1)}, u32[]{:S(2)}, u32[]{:S(2)}) %collective-permute-start.2) | collective-permute-done | bytes 1048608 | tf_op jit(solution)/shard_map/ppermute | solution.py:18
  98.9 2.1 %fusion.64 = (f32[16,4,32]{2,1,0:T(4,128)S(1)}, f32[16,4,32,160]{3,2,1,0:T(8,128)S(1)}) fusion(bf16[32,16,4,128]{3,2,1,0:T(4,128)(2,1)S(1)} %bitcast.92, bf16[160,16,4,128]{3,1,0,2:T(8,128)(2,1)S(1)} %bitcast.84, pred[32,160]{1,0:T(8,128)(4,1)S(1)} %fusion.56), kind=kOutput, calls=%fused_computation.82 | convolution fusion | flops 84867072 | bytes 4469760 | tf_op jit(solution)/shard_map/qrhd,krhd->rhqk/dot_general | solution.py:33
  103.4 2.8 %pad_maximum_fusion.1 = bf16[2560,4,128]{0,2,1:T(8,128)(2,1)} fusion(bf16[512,4,128]{0,2,1:T(8,128)(2,1)S(1)} %copy.68, bf16[512,4,128]{0,2,1:T(8,128)(2,1)} %collective-permute-done.3, bf16[1024,4,128]{0,2,1:T(8,128)(2,1)} %collective-permute-done.5, bf16[512,4,128]{0,2,1:T(8,128)(2,1)} %collective-permute-done.4), kind=kLoop, calls=%fused_computation.9 | loop fusion | flops 10485760 | bytes 5242880 | tf_op jit(solution)/shard_map/concatenate | solution.py:76
  106.3 4.4 %copy.77 = bf16[2560,4,128]{2,0,1:T(8,128)(2,1)} copy(bf16[2560,4,128]{0,2,1:T(8,128)(2,1)} %pad_maximum_fusion.1) | data formatting | bytes 5242880 | tf_op jit(solution)/shard_map/concatenate | solution.py:76
  110.7 4.3 %fusion.31 = f32[32,16,4,128]{3,0,2,1:T(8,128)S(1)} fusion(bf16[160,16,4,128]{3,1,0,2:T(8,128)(2,1)} %bitcast.85, f32[16,4,32,160]{3,2,1,0:T(8,128)} %copy-done.2, f32[16,4,32]{2,1,0:T(4,128)S(1)} %get-tuple-element.5, f32[32,16,4]{0,2,1:T(4,128)S(1)} %bitcast.88), kind=kOutput, calls=%fused_computation.36 | convolution fusion | flops 84803584 | bytes 4997120 | tf_op jit(solution)/shard_map/rhqk,krhd->qrhd/dot_general | solution.py:48
  116.5 2.5 %copy.81 = f32[1,512,4,128]{1,3,2,0:T(8,128)} copy(f32[1,512,4,128]{3,1,2,0:T(8,128)} %bitcast.83) | data formatting | bytes 2097152 | tf_op jit(solution)/shard_map/stack;reshape | solution.py:93
  119.2 2.9 %fusion.3 = bf16[512,4,128]{0,2,1:T(8,128)(2,1)} fusion(f32[1,512,4,128]{1,3,2,0:T(8,128)} %copy.81, f32[1,512,4,128]{1,3,2,0:T(8,128)S(1)} %copy-done.1, f32[1,512,4,128]{1,3,2,0:T(8,128)} %divide_bitcast_fusion, f32[3,512,4]{1,2,0:T(4,128)S(1)} %broadcast_divide_fusion), kind=kLoop, calls=%fused_computation.6 | loop fusion | flops 2883584 | bytes 3694592 | tf_op jit(solution)/shard_map/reduce_sum | solution.py:92
  122.1 25.8 %all-gather.2.cloned.1.call-done = bf16[512,1024]{0,1:T(8,128)(2,1)} async-done(((bf16[512,512]{0,1:T(8,128)(2,1)}), bf16[512,1024]{0,1:T(8,128)(2,1)}) %all-gather.2.cloned.1.call-update) | async-done | bytes 1048592 | tf_op jit(solution)/shard_map/all_gather | solution.py:97
  147.9 3.5 %convolution_convert_fusion = bf16[512,1024]{1,0:T(8,128)(2,1)} fusion(bf16[512,1024]{0,1:T(8,128)(2,1)} %all-gather.2.cloned.1.call-done, bf16[1024,1024]{1,0:T(8,128)(2,1)S(1)} %copy-done), kind=kOutput, calls=%fused_computation.26 | convolution fusion | flops 1074266112 | bytes 4194304 | tf_op jit(solution)/shard_map/dot_general | solution.py:96
  (48 shorter events, 16.1 us)
Async XLA Ops:
  6.5 141.4 %copy-start = (bf16[1024,1024]{1,0:T(8,128)(2,1)S(1)}, bf16[1024,1024]{1,0:T(8,128)(2,1)}, u32[]{:S(2)}) copy-start(bf16[1024,1024]{1,0:T(8,128)(2,1)} %param.7) | copy-start | bytes 6291460
  6.5 141.4 %all-gather.2.cloned.1.call-start = ((), (), s32[]{:S(2)}) async-start(), calls=%async_computation | async-start | bytes 1572864 | tf_op jit(solution)/shard_map/all_gather | solution.py:97
  7.8 86.6 %collective-permute-start.1 = (bf16[512,4,128]{2,0,1:T(8,128)(2,1)S(1)}, bf16[512,4,128]{2,0,1:T(8,128)(2,1)}, u32[]{:S(2)}, u32[]{:S(2)}) collective-permute-start(bf16[512,4,128]{2,0,1:T(8,128)(2,1)S(1)} %copy.55), channel_id=1, source_target_pairs={{0,8},{2,10},{4,12},{6,14},{8,16},{10,18},{12,20},{14,22},{16,24},... | collective-permute-start | bytes 1572872 | tf_op jit(solution)/shard_map/ppermute | solution.py:18
  13.6 36.4 %collective-permute-start = (bf16[512,4,128]{2,0,1:T(8,128)(2,1)S(1)}, bf16[512,4,128]{2,0,1:T(8,128)(2,1)}, u32[]{:S(2)}, u32[]{:S(2)}) collective-permute-start(bf16[512,4,128]{2,0,1:T(8,128)(2,1)S(1)} %copy.55), channel_id=1, source_target_pairs={{0,2},{2,4},{4,6},{6,8},{8,10},{10,12},{12,14},{14,16},{16,18},{18... | collective-permute-start | bytes 1572872 | tf_op jit(solution)/shard_map/ppermute | solution.py:18
  19.1 84.3 %collective-permute-start.4 = (bf16[512,4,128]{0,2,1:T(8,128)(2,1)S(1)}, bf16[512,4,128]{0,2,1:T(8,128)(2,1)}, u32[]{:S(2)}, u32[]{:S(2)}) collective-permute-start(bf16[512,4,128]{0,2,1:T(8,128)(2,1)S(1)} %copy.68), channel_id=1, source_target_pairs={{0,8},{2,10},{4,12},{6,14},{8,16},{10,18},{12,20},{14,22},{16,24},... | collective-permute-start | bytes 1572872 | tf_op jit(solution)/shard_map/ppermute | solution.py:18
  21.8 17.3 %collective-permute-start.3 = (bf16[512,4,128]{0,2,1:T(8,128)(2,1)S(1)}, bf16[512,4,128]{0,2,1:T(8,128)(2,1)}, u32[]{:S(2)}, u32[]{:S(2)}) collective-permute-start(bf16[512,4,128]{0,2,1:T(8,128)(2,1)S(1)} %copy.68), channel_id=1, source_target_pairs={{0,2},{2,4},{4,6},{6,8},{8,10},{10,12},{12,14},{14,16},{16,18},{18... | collective-permute-start | bytes 1572872 | tf_op jit(solution)/shard_map/ppermute | solution.py:18
  43.5 59.9 %collective-permute-start.5 = (bf16[1024,4,128]{0,2,1:T(8,128)(2,1)}, bf16[1024,4,128]{0,2,1:T(8,128)(2,1)}, u32[]{:S(2)}, u32[]{:S(2)}) collective-permute-start(bf16[1024,4,128]{0,2,1:T(8,128)(2,1)} %pad_maximum_fusion.2), channel_id=1, source_target_pairs={{0,4},{2,6},{4,8},{6,10},{8,12},{10,14},{12,16},{14,18},{16,20},{1... | collective-permute-start | bytes 3145736 | tf_op jit(solution)/shard_map/ppermute | solution.py:18
  53.9 43.4 %collective-permute-start.2 = (bf16[1024,4,128]{2,0,1:T(8,128)(2,1)}, bf16[1024,4,128]{2,0,1:T(8,128)(2,1)}, u32[]{:S(2)}, u32[]{:S(2)}) collective-permute-start(bf16[1024,4,128]{2,0,1:T(8,128)(2,1)} %constant_dynamic-update-slice_fusion), channel_id=1, source_target_pairs={{0,4},{2,6},{4,8},{6,10},{8,12},{10,14},{12,16},{14,18},{16,20},{1... | collective-permute-start | bytes 3145736 | tf_op jit(solution)/shard_map/ppermute | solution.py:18
  78.6 1.4 copy-start.3
  87.4 2.4 %copy-start.4 = (pred[512,640]{0,1:T(8,128)(4,1)S(1)}, pred[512,640]{0,1:T(8,128)(4,1)}, u32[]{:S(2)}) copy-start(pred[512,640]{0,1:T(8,128)(4,1)} %fusion.30) | copy-start | bytes 983044
  94.4 4.5 %copy-start.5 = (bf16[512,4,128]{2,1,0:T(4,128)(2,1)S(1)}, bf16[512,4,128]{2,1,0:T(4,128)(2,1)}, u32[]{:S(2)}) copy-start(bf16[512,4,128]{2,1,0:T(4,128)(2,1)} %param.4) | copy-start | bytes 1572868
  101.0 1.4 copy-start.2
  114.9 4.2 %copy-start.1 = (f32[1,512,4,128]{1,3,2,0:T(8,128)S(1)}, f32[1,512,4,128]{1,3,2,0:T(8,128)}, u32[]{:S(2)}) copy-start(f32[1,512,4,128]{1,3,2,0:T(8,128)} %copy.80) | copy-start | bytes 3145732
Sparse Core Ops, SparseCore 0:
  122.2 25.6 all-gather.1
where the time goes:
time: 159 us; the launch traced here: 158 us
  starting transfers between devices  46.2 us (29%)
  waiting for transfers between devices  40.5 us (25%)
  local copies, waits for them, and re-layouts  24.7 us (16%)
  matrix products  20.3 us (13%)
  between operations  13.6 us (9%)
  other arithmetic  13.1 us (8%)
    ppermute x6, starting transfers between devices, from_behind(): return lax.ppermute(block, axis, route)  46.2 us
    all_gather x1, waiting for transfers between devices, local(): lax.all_gather(attended, 'tp', axis=1, tiled=True)  25.8 us
    ppermute x6, waiting for transfers between devices, from_behind(): return lax.ppermute(block, axis, route)  14.7 us
    dot_general x3, matrix products, branch_attend(): jnp.einsum('rhqk,krhd->qrhd', numerators.astype(jnp.bfloat16), value_res,...  10.4 us
    unnamed x15, local copies, waits for them, and re-layouts  6.95 us
    concatenate x2, local copies, waits for them, and re-layouts, local(): value_holder = jnp.concatenate([moved_values, value_holder], axis=0)  6.66 us
    dot_general x3, matrix products, branch_attend(): jnp.einsum('qrhd,krhd->rhqk', query_res, key_res, preferred_element_type=...  6.41 us
    another operation x2, local copies, waits for them, and re-layouts, local(): jnp.stack([first_out, second_output, third_output])  5.09 us
  transfers between devices with their start and end apart: 7, of which 3 were waited for; matrix products, arithmetic and copies ran while one was open for 20% of the time, Pallas kernels for 0%

commit v1 on v0

v1 whole, which is shorter than its diff:
```python
import functools
import math

import jax
import jax.numpy as jnp
from jax import lax
from jax.experimental import pallas as pl
from jax.experimental.pallas import tpu as pltpu
from jax.sharding import PartitionSpec as P

W1 = 128
WINDOW_TWO = 512
DILATION_TWO = 4
WINDOW_THREE = 2048
DILATION_THREE = 16
MESH = pl.DeviceIdType.MESH
RATIO = DILATION_THREE // DILATION_TWO
CHUNKS = DILATION_TWO
ROWS_ONE = 16
ROWS_TWO = WINDOW_TWO // DILATION_THREE


def attend(queries, keys, values, bias, scale):
    scores = lax.dot_general(
        queries, keys, (((1,), (1,)), ((), ())), preferred_element_type=jnp.float32
    )
    scores = scores * scale + bias
    top = jnp.max(scores, axis=-1, keepdims=True)
    numerators = jnp.exp2(scores - top)
    total = jnp.sum(numerators, axis=-1, keepdims=True)
    weighted = jnp.dot(numerators.astype(jnp.bfloat16), values, preferred_element_type=jnp.float32)
    return weighted, top, total


def bias_of(shape, place_q, place_k, first_own, window, has_prev):
    query_place, _ = place_q(lax.broadcasted_iota(jnp.int32, shape, 0))
    key_place, key_row = place_k(lax.broadcasted_iota(jnp.int32, shape, 1))
    distance = query_place - key_place
    allowed = (distance >= 0) & (distance <= window)
    general = jnp.where(allowed, 0.0, -jnp.inf).astype(jnp.float32)
    gate = jnp.where(has_prev, 0, first_own)
    first = jnp.where(allowed & (key_row >= gate), 0.0, -jnp.inf).astype(jnp.float32)
    return general, first


def kernel(
    group, q_ref, k_ref, v_ref, w_ref, o_ref,
    qb, kb, vb, acc, mx, sm, ob, ab, bias1, bias1f, bias2, bias2f, bias3,
    in_send, in_recv, z_send, z_recv, zl_send, zl_recv, o_send, o_recv, d_send, d_recv,
):
    res, dim = DILATION_THREE, q_ref.shape[-1]
    piece = q_ref.shape[2]
    rows = group * piece
    sp, tp = lax.axis_index("sp"), lax.axis_index("tp")
    n_sp, n_tp = lax.axis_size("sp"), lax.axis_size("tp")
    mine = lax.rem(sp, group)
    base = sp - mine
    has_prev = sp >= group
    has_next = sp + group < n_sp
    partner = n_tp - 1 - tp
    scale = math.log2(math.e) / math.sqrt(dim)

    barrier = pltpu.get_barrier_semaphore()
    for d in range(1, group):
        pl.semaphore_signal(
            barrier, inc=1, device_id={"sp": base + lax.rem(mine + d, group)}, device_id_type=MESH
        )
    pl.semaphore_signal(barrier, inc=1, device_id={"tp": partner}, device_id_type=MESH)

    @pl.when(has_prev)
    def _():
        pl.semaphore_signal(barrier, inc=1, device_id={"sp": sp - group}, device_id_type=MESH)

    @pl.when(has_next)
    def _():
        pl.semaphore_signal(barrier, inc=1, device_id={"sp": sp + group}, device_id_type=MESH)

    pl.semaphore_wait(barrier, group + jnp.where(has_prev, 1, 0) + jnp.where(has_next, 1, 0))

    def span(start):
        return pl.ds(pl.multiple_of(start, piece), piece)

    tensors = ((k_ref, kb, rows), (v_ref, vb, rows), (q_ref, qb, 0))

    def exchange(which, d):
        source, buffer, offset = tensors[which]
        other = lax.rem(mine + d, group)
        return pltpu.make_async_remote_copy(
            src_ref=source.at[other],
            dst_ref=buffer.at[:, span(offset + piece * mine), :],
            send_sem=in_send.at[which, d],
            recv_sem=in_recv.at[which, mine],
            device_id={"sp": base + other},
            device_id_type=MESH,
        )

    def arrival(which, origin):
        source, buffer, offset = tensors[which]
        return pltpu.make_async_remote_copy(
            src_ref=source.at[0],
            dst_ref=buffer.at[:, span(offset + piece * origin), :],
            send_sem=in_send.at[which, 0],
            recv_sem=in_recv.at[which, origin],
            device_id={"sp": sp},
            device_id_type=MESH,
        )

    def order(k):
        if k == 0:
            return mine
        high = group - k
        return jnp.where(high > mine, high, high - 1)

    def onward(which, k):
        source, buffer, _ = tensors[which]
        origin = order(k)
        src = source.at[mine] if k == 0 else buffer.at[:, span(rows + piece * origin), :]
        return pltpu.make_async_remote_copy(
            src_ref=src,
            dst_ref=buffer.at[:, span(piece * origin), :],
            send_sem=z_send.at[which, k],
            recv_sem=z_recv.at[which, k],
            device_id={"sp": sp + group},
            device_id_type=MESH,
        )

    def onward_last(which, s):
        _, buffer, _ = tensors[which]
        origin = order(group - 1)
        part = pl.ds(s * RATIO, RATIO)
        return pltpu.make_async_remote_copy(
            src_ref=buffer.at[part, span(rows + piece * origin), :],
            dst_ref=buffer.at[part, span(piece * origin), :],
            send_sem=zl_send.at[which, s],
            recv_sem=zl_recv.at[which, s],
            device_id={"sp": sp + group},
            device_id_type=MESH,
        )

    @pl.when(has_next)
    def _():
        for which in (0, 1):
            onward(which, 0).start()

    for which in (0, 1, 2):
        for d in range(1, group):
            exchange(which, d).start()

    for source, buffer, offset in tensors:
        buffer[:, span(offset + piece * mine), :] = source[mine]

    @pl.when(jnp.logical_not(has_prev))
    def _():
        kb[:, :rows, :] = jnp.zeros((res, rows, dim), kb.dtype)
        vb[:, :rows, :] = jnp.zeros((res, rows, dim), vb.dtype)

    def place_one(per):
        def place(i):
            store, row = i // per, i % per
            residue = (store % RATIO) * DILATION_TWO + store // RATIO
            return row * res + residue, row
        return place

    def place_two(per):
        def place(i):
            j, row = i // per, i % per
            return row * RATIO + j, row
        return place

    def shifted(place, by):
        def moved(i):
            at, row = place(i)
            return at + by, row
        return moved

    bias1[...], bias1f[...] = bias_of(
        bias1.shape, shifted(place_one(ROWS_ONE), ROWS_ONE * res), place_one(2 * ROWS_ONE), ROWS_ONE, W1, has_prev
    )
    bias2[...], bias2f[...] = bias_of(
        bias2.shape, shifted(place_two(ROWS_TWO), ROWS_TWO * RATIO), place_two(2 * ROWS_TWO), ROWS_TWO,
        WINDOW_TWO // DILATION_TWO, has_prev,
    )
    _, bias3[...] = bias_of(
        bias3.shape, lambda i: (i + rows, i), lambda i: (i, i), rows, WINDOW_THREE // DILATION_THREE, has_prev
    )

    for k in range(1, group):
        origin = order(k)
        for which in (0, 1):
            arrival(which, origin).wait_recv()

        @pl.when(has_next)
        def _():
            if k < group - 1:
                for which in (0, 1):
                    onward(which, k).start()
            else:
                for s in range(CHUNKS):
                    for which in (0, 1):
                        onward_last(which, s).start()

    for k in range(1, group):
        arrival(2, order(k)).wait_recv()

    def branch_one(b, bias):
        own = pl.ds(b * ROWS_ONE, ROWS_ONE)
        near = pl.ds(rows + (b - 1) * ROWS_ONE, 2 * ROWS_ONE)
        weighted, top, total = attend(
            qb[:, own, :].reshape(-1, dim), kb[:, near, :].reshape(-1, dim), vb[:, near, :].reshape(-1, dim),
            bias[...], scale,
        )
        acc[:, own, :] = weighted.reshape(res, ROWS_ONE, dim)
        mx[:, own, :] = top.reshape(res, ROWS_ONE, 1)
        sm[:, own, :] = total.reshape(res, ROWS_ONE, 1)

    def merge(at, weighted, top, total):
        old_top = mx[at].reshape(-1, 1)
        new_top = jnp.maximum(old_top, top)
        old_part, part = jnp.exp2(old_top - new_top), jnp.exp2(top - new_top)
        return (
            acc[at].reshape(-1, dim) * old_part + weighted * part,
            new_top,
            sm[at].reshape(-1, 1) * old_part + total * part,
        )

    def branch_two(s, b, bias):
        part = pl.ds(s * RATIO, RATIO)
        own = pl.ds(b * ROWS_TWO, ROWS_TWO)
        near = pl.ds(rows + (b - 1) * ROWS_TWO, 2 * ROWS_TWO)
        found = attend(
            qb[part, own, :].reshape(-1, dim), kb[part, near, :].reshape(-1, dim), vb[part, near, :].reshape(-1, dim),
            bias[...], scale,
        )
        at = (part, own, slice(None))
        weighted, top, total = merge(at, *found)
        acc[at] = weighted.reshape(RATIO, ROWS_TWO, dim)
        mx[at] = top.reshape(RATIO, ROWS_TWO, 1)
        sm[at] = total.reshape(RATIO, ROWS_TWO, 1)

    for b in range(1, rows // ROWS_ONE):
        branch_one(b, bias1)
    for s in range(CHUNKS):
        for b in range(1, rows // ROWS_TWO):
            branch_two(s, b, bias2)

    @pl.when(has_prev)
    def _():
        for k in range(group - 1):
            for which in (0, 1):
                onward(which, k).wait_recv()

    branch_one(0, bias1f)
    for s in range(CHUNKS):
        branch_two(s, 0, bias2f)

    head = tp * group + mine

    def lanes(index):
        return pl.ds(pl.multiple_of(index * dim, dim), dim)

    def give(s, d):
        part = pl.ds(s * RATIO, RATIO)
        other = lax.rem(mine + d, group)
        return pltpu.make_async_remote_copy(
            src_ref=ob.at[part, span(piece * other), :],
            dst_ref=ab.at[part, :, lanes(head)],
            send_sem=o_send.at[s, d],
            recv_sem=o_recv.at[s, mine],
            device_id={"sp": base + other},
            device_id_type=MESH,
        )

    def taken(s, origin):
        part = pl.ds(s * RATIO, RATIO)
        return pltpu.make_async_remote_copy(
            src_ref=ob.at[part, span(0), :],
            dst_ref=ab.at[part, :, lanes(tp * group + origin)],
            send_sem=o_send.at[s, 0],
            recv_sem=o_recv.at[s, origin],
            device_id={"sp": sp},
            device_id_type=MESH,
        )

    def swap(s, d):
        part = pl.ds(s * RATIO, RATIO)
        origin = lax.rem(mine + d, group)
        slot = ab.at[part, :, lanes(tp * group + origin)]
        return pltpu.make_async_remote_copy(
            src_ref=ob.at[part, span(piece * mine), :] if d == 0 else slot,
            dst_ref=slot,
            send_sem=d_send.at[s, d],
            recv_sem=d_recv.at[s, d],
            device_id={"tp": partner},
            device_id_type=MESH,
        )

    def swapped(s, d):
        part = pl.ds(s * RATIO, RATIO)
        origin = lax.rem(mine + d, group)
        return pltpu.make_async_remote_copy(
            src_ref=ob.at[part, span(0), :],
            dst_ref=ab.at[part, :, lanes(partner * group + origin)],
            send_sem=d_send.at[s, d],
            recv_sem=d_recv.at[s, d],
            device_id={"tp": partner},
            device_id_type=MESH,
        )

    for s in range(CHUNKS):
        part = pl.ds(s * RATIO, RATIO)

        @pl.when(has_prev)
        def _():
            for which in (0, 1):
                onward_last(which, s).wait_recv()

        for store in range(s * RATIO, (s + 1) * RATIO):
            found = attend(qb[store], kb[store], vb[store], bias3[...], scale)
            weighted, _, total = merge((store,), *found)
            ob[store] = (weighted / total).astype(ob.dtype)
        for d in range(1, group):
            give(s, d).start()
        swap(s, 0).start()
        ab[part, :, lanes(head)] = ob[part, span(piece * mine), :]

    for s in range(CHUNKS):
        part = pl.ds(s * RATIO, RATIO)
        for d in range(1, group):
            taken(s, lax.rem(mine + d, group)).wait_recv()
            swap(s, d).start()
    for s in range(CHUNKS):
        part = pl.ds(s * RATIO, RATIO)
        for d in range(group):
            swapped(s, d).wait_recv()
        attended = ab[part].reshape(RATIO * piece, -1)
        mixed = jnp.dot(attended, w_ref[...], preferred_element_type=jnp.float32)
        o_ref[part] = mixed.astype(o_ref.dtype).reshape(RATIO, piece, -1)

    for which in (0, 1, 2):
        for d in range(1, group):
            exchange(which, d).wait_send()

    @pl.when(has_next)
    def _():
        for which in (0, 1):
            for k in range(group - 1):
                onward(which, k).wait_send()
            for s in range(CHUNKS):
                onward_last(which, s).wait_send()

    for s in range(CHUNKS):
        for d in range(1, group):
            give(s, d).wait_send()
        for d in range(group):
            swap(s, d).wait_send()


def local(queries, keys, values, w_out):
    tokens, group, dim = queries.shape
    features, columns = w_out.shape
    res = DILATION_THREE
    piece = tokens // res
    rows = group * piece
    assert group * tokens == WINDOW_THREE and lax.axis_size("sp") % group == 0 and lax.axis_size("tp") == 2

    def by_residue(x):
        x = x.reshape(piece, RATIO, DILATION_TWO, group, dim)
        return jnp.transpose(x, (3, 2, 1, 0, 4)).reshape(group, res, piece, dim)

    low, full = jnp.bfloat16, jnp.float32
    dma = pltpu.SemaphoreType.DMA
    vmem = pl.BlockSpec(memory_space=pltpu.VMEM)
    mixed = pl.pallas_call(
        functools.partial(kernel, group),
        out_shape=jax.ShapeDtypeStruct((res, piece, columns), low),
        in_specs=[vmem] * 4,
        out_specs=vmem,
        scratch_shapes=[
            pltpu.VMEM((res, rows, dim), low),
            pltpu.VMEM((res, 2 * rows, dim), low),
            pltpu.VMEM((res, 2 * rows, dim), low),
            pltpu.VMEM((res, rows, dim), full),
            pltpu.VMEM((res, rows, 1), full),
            pltpu.VMEM((res, rows, 1), full),
            pltpu.VMEM((res, rows, dim), low),
            pltpu.VMEM((res, piece, features), low),
            pltpu.VMEM((res * ROWS_ONE, 2 * res * ROWS_ONE), full),
            pltpu.VMEM((res * ROWS_ONE, 2 * res * ROWS_ONE), full),
            pltpu.VMEM((RATIO * ROWS_TWO, 2 * RATIO * ROWS_TWO), full),
            pltpu.VMEM((RATIO * ROWS_TWO, 2 * RATIO * ROWS_TWO), full),
            pltpu.VMEM((rows, 2 * rows), full),
            dma((3, group)), dma((3, group)),
            dma((2, group)), dma((2, group)),
            dma((2, CHUNKS)), dma((2, CHUNKS)),
            dma((CHUNKS, group)), dma((CHUNKS, group)),
            dma((CHUNKS, group)), dma((CHUNKS, group)),
        ],
        compiler_params=pltpu.CompilerParams(
            collective_id=0, has_side_effects=True, vmem_limit_bytes=48 * 2**20
        ),
    )(by_residue(queries), by_residue(keys), by_residue(values), w_out)
    mixed = mixed.reshape(DILATION_TWO, RATIO, piece, columns)
    return jnp.transpose(mixed, (2, 1, 0, 3)).reshape(tokens, columns)


def solution(mesh):
    in_specs = (P("sp", "tp", None), P("sp", "tp", None), P("sp", "tp", None), P(None, "tp"))
    out_specs = P("sp", "tp")
    return jax.shard_map(local, mesh=mesh, in_specs=in_specs, out_specs=out_specs, check_vma=False)
```

time: 159 us -> 50.1 us (0.32)
  the two profiles are of different devices: /device:TPU:0 before, /device:TPU:19 now
where the time goes in v1:
time: 50.1 us; the launch traced here: 49.9 us
  Pallas kernels  43.6 us (87%)
  local copies, waits for them, and re-layouts  6.23 us (12%)
    pallas_call x1, Pallas kernels, local(): pl.pallas_call(functools.partial(kernel, group), out_shape=jax.ShapeDtype...  43.6 us
    reshape x3, local copies, waits for them, and re-layouts, by_residue(): x = x.reshape(piece, RATIO, DILATION_TWO, group, dim)  4.31 us
    reshape x1, local copies, waits for them, and re-layouts, local(): return jnp.transpose(mixed, (2, 1, 0, 3)).reshape(tokens, columns)  1.11 us

profile of v1, /device:TPU:19, one launch (start us, length us, event | category | flops | bytes accessed | tf_op | source)
XLA Modules:
  0.0 49.9 jit_solution(8096019593535724613)
XLA Ops:
  0.0 0.0 copy-start
  0.0 1.5 %copy.5 = bf16[32,4,4,4,128]{4,0,1,2,3:T(8,128)(2,1)S(1)} copy(bf16[32,4,4,4,128]{4,3,2,1,0:T(4,128)(2,1)} %bitcast.19) | data formatting | bytes 1048576 | tf_op jit(solution)/shard_map/reshape | solution.py:367
  1.5 1.4 %copy.6 = bf16[32,4,4,4,128]{4,0,1,2,3:T(8,128)(2,1)S(1)} copy(bf16[32,4,4,4,128]{4,3,2,1,0:T(4,128)(2,1)} %bitcast.20) | data formatting | bytes 1048576 | tf_op jit(solution)/shard_map/reshape | solution.py:367
  2.9 1.4 %copy.7 = bf16[32,4,4,4,128]{4,0,1,2,3:T(8,128)(2,1)S(1)} copy(bf16[32,4,4,4,128]{4,3,2,1,0:T(4,128)(2,1)} %bitcast.21) | data formatting | bytes 1048576 | tf_op jit(solution)/shard_map/reshape | solution.py:367
  4.3 0.0 copy-done
  4.3 43.6 %shard_map.46 = bf16[16,32,1024]{2,1,0:T(8,128)(2,1)S(1)} custom-call(bf16[4,16,32,128]{3,2,1,0:T(8,128)(2,1)S(1)} %bitcast.16, bf16[4,16,32,128]{3,2,1,0:T(8,128)(2,1)S(1)} %bitcast.17, bf16[4,16,32,128]{3,2,1,0:T(8,128)(2,1)S(1)} %bitcast.18, bf16[1024,1024]{1,0:T(8,128)(2,1)S(1)} %copy-done), custom_call_target="tpu_custom_call" | custom-call | tf_op jit(solution)/shard_map/pallas_call | solution.py:373
  48.0 0.8 %copy.8 = bf16[32,4,4,1024]{3,2,1,0:T(4,128)(2,1)S(1)} copy(bf16[32,4,4,1024]{3,0,1,2:T(8,128)(2,1)S(1)} %bitcast.15) | data formatting | bytes 2097152 | tf_op jit(solution)/shard_map/transpose | solution.py:403
  48.8 1.1 %reshape.31 = bf16[512,1024]{1,0:T(8,128)(2,1)} reshape(bf16[32,4,4,1024]{3,2,1,0:T(4,128)(2,1)S(1)} %copy.8) | data formatting | bytes 2097152 | tf_op jit(solution)/shard_map/reshape | solution.py:403
Async XLA Ops:
  0.0 4.3 %copy-start = (bf16[1024,1024]{1,0:T(8,128)(2,1)S(1)}, bf16[1024,1024]{1,0:T(8,128)(2,1)}, u32[]{:S(2)}) copy-start(bf16[1024,1024]{1,0:T(8,128)(2,1)} %w_ref.1) | copy-start | bytes 6291460

commit v2 on v1

--- a/solution.py
+++ b/solution.py
@@ -20,16 +20,20 @@
 ROWS_TWO = WINDOW_TWO // DILATION_THREE
 
 
-def attend(queries, keys, values, bias, scale):
-    scores = lax.dot_general(
-        queries, keys, (((1,), (1,)), ((), ())), preferred_element_type=jnp.float32
-    )
-    scores = scores * scale + bias
-    top = jnp.max(scores, axis=-1, keepdims=True)
-    numerators = jnp.exp2(scores - top)
-    total = jnp.sum(numerators, axis=-1, keepdims=True)
-    weighted = jnp.dot(numerators.astype(jnp.bfloat16), values, preferred_element_type=jnp.float32)
-    return weighted, top, total
+def attend(blocks, scale):
+    scores = [
+        lax.dot_general(q, k, (((1,), (1,)), ((), ())), preferred_element_type=jnp.float32)
+        for q, k, _, _ in blocks
+    ]
+    scores = [x * scale + bias for x, (_, _, _, bias) in zip(scores, blocks)]
+    tops = [jnp.max(x, axis=-1, keepdims=True) for x in scores]
+    numerators = [jnp.exp2(x - top) for x, top in zip(scores, tops)]
+    totals = [jnp.sum(x, axis=-1, keepdims=True) for x in numerators]
+    weighted = [
+        jnp.dot(x.astype(jnp.bfloat16), v, preferred_element_type=jnp.float32)
+        for x, (_, _, v, _) in zip(numerators, blocks)
+    ]
+    return list(zip(weighted, tops, totals))
 
 
 def bias_of(shape, place_q, place_k, first_own, window, has_prev):
@@ -82,69 +86,86 @@
 
     tensors = ((k_ref, kb, rows), (v_ref, vb, rows), (q_ref, qb, 0))
 
+    def member(d):
+        other, bit = mine, 1
+        while bit <= d:
+            if d & bit:
+                other = other + bit * (1 - 2 * lax.rem(mine // bit, 2))
+            bit *= 2
+        return other
+
     def exchange(which, d):
         source, buffer, offset = tensors[which]
-        other = lax.rem(mine + d, group)
+        other = member(d)
         return pltpu.make_async_remote_copy(
             src_ref=source.at[other],
             dst_ref=buffer.at[:, span(offset + piece * mine), :],
             send_sem=in_send.at[which, d],
-            recv_sem=in_recv.at[which, mine],
+            recv_sem=in_recv.at[which, d],
             device_id={"sp": base + other},
             device_id_type=MESH,
         )
 
-    def arrival(which, origin):
+    def arrival(which, d):
         source, buffer, offset = tensors[which]
         return pltpu.make_async_remote_copy(
             src_ref=source.at[0],
-            dst_ref=buffer.at[:, span(offset + piece * origin), :],
-            send_sem=in_send.at[which, 0],
-            recv_sem=in_recv.at[which, origin],
+            dst_ref=buffer.at[:, span(offset + piece * member(d)), :],
+            send_sem=in_send.at[which, d],
+            recv_sem=in_recv.at[which, d],
             device_id={"sp": sp},
             device_id_type=MESH,
         )
 
-    def order(k):
+    low = piece - ROWS_ONE
+
+    def onward_rows(which, k):
+        source, buffer, _ = tensors[which]
+        start = piece * member(k)
         if k == 0:
-            return mine
-        high = group - k
-        return jnp.where(high > mine, high, high - 1)
-
-    def onward(which, k):
-        source, buffer, _ = tensors[which]
-        origin = order(k)
-        src = source.at[mine] if k == 0 else buffer.at[:, span(rows + piece * origin), :]
+            src, dst = source.at[mine], buffer.at[:, span(start), :]
+        elif k in whole:
+            src, dst = buffer.at[:, span(rows + start), :], buffer.at[:, span(start), :]
+        else:
+            ends = [pl.ds(pl.multiple_of(x + start + low, ROWS_ONE), ROWS_ONE) for x in (rows, 0)]
+            src, dst = (buffer.at[:, x, :] for x in ends)
         return pltpu.make_async_remote_copy(
             src_ref=src,
-            dst_ref=buffer.at[:, span(piece * origin), :],
+            dst_ref=dst,
             send_sem=z_send.at[which, k],
             recv_sem=z_recv.at[which, k],
             device_id={"sp": sp + group},
             device_id_type=MESH,
         )
 
-    def onward_last(which, s):
+    def onward_chunk(which, k, s):
         _, buffer, _ = tensors[which]
-        origin = order(group - 1)
-        part = pl.ds(s * RATIO, RATIO)
-        return pltpu.make_async_remote_copy(
-            src_ref=buffer.at[part, span(rows + piece * origin), :],
-            dst_ref=buffer.at[part, span(piece * origin), :],
-            send_sem=zl_send.at[which, s],
-            recv_sem=zl_recv.at[which, s],
+        start = piece * member(k)
+        part = pl.ds(s * RATIO, RATIO)
+        return pltpu.make_async_remote_copy(
+            src_ref=buffer.at[part, pl.ds(pl.multiple_of(rows + start, ROWS_ONE), low), :],
+            dst_ref=buffer.at[part, pl.ds(pl.multiple_of(start, ROWS_ONE), low), :],
+            send_sem=zl_send.at[which, k, s],
+            recv_sem=zl_recv.at[which, k, s],
             device_id={"sp": sp + group},
             device_id_type=MESH,
         )
 
+    whole = range(group // 2)
+    split = range(group // 2, group)
+
     @pl.when(has_next)
     def _():
         for which in (0, 1):
-            onward(which, 0).start()
-
-    for which in (0, 1, 2):
-        for d in range(1, group):
-            exchange(which, d).start()
+            onward_rows(which, 0).start()
+
+    near = [d for d in range(1, group) if d & (d - 1) == 0]
+    far = [d for d in range(1, group) if d & (d - 1)]
+    for tensors_now in ((0, 1), (2,)):
+        for members in (near, far):
+            for which in tensors_now:
+                for d in members:
+                    exchange(which, d).start()
 
     for source, buffer, offset in tensors:
         buffer[:, span(offset + piece * mine), :] = source[mine]
@@ -185,33 +206,39 @@
     )
 
     for k in range(1, group):
-        origin = order(k)
         for which in (0, 1):
-            arrival(which, origin).wait_recv()
+            arrival(which, k).wait_recv()
 
         @pl.when(has_next)
         def _():
-            if k < group - 1:
+            for which in (0, 1):
+                onward_rows(which, k).start()
+
+    @pl.when(has_next)
+    def _():
+        for s in range(CHUNKS):
+            for k in split:
                 for which in (0, 1):
-                    onward(which, k).start()
-            else:
-                for s in range(CHUNKS):
-                    for which in (0, 1):
-                        onward_last(which, s).start()
+                    onward_chunk(which, k, s).start()
 
     for k in range(1, group):
-        arrival(2, order(k)).wait_recv()
-
-    def branch_one(b, bias):
-        own = pl.ds(b * ROWS_ONE, ROWS_ONE)
-        near = pl.ds(rows + (b - 1) * ROWS_ONE, 2 * ROWS_ONE)
-        weighted, top, total = attend(
-            qb[:, own, :].reshape(-1, dim), kb[:, near, :].reshape(-1, dim), vb[:, near, :].reshape(-1, dim),
-            bias[...], scale,
-        )
-        acc[:, own, :] = weighted.reshape(res, ROWS_ONE, dim)
-        mx[:, own, :] = top.reshape(res, ROWS_ONE, 1)
-        sm[:, own, :] = total.reshape(res, ROWS_ONE, 1)
+        arrival(2, k).wait_recv()
+
+    def branch_one(blocks, bias):
+        spans = [
+            (pl.ds(b * ROWS_ONE, ROWS_ONE), pl.ds(rows + (b - 1) * ROWS_ONE, 2 * ROWS_ONE)) for b in blocks
+        ]
+        found = attend(
+            [
+                tuple(x[:, at, :].reshape(-1, dim) for x, at in ((qb, own), (kb, near), (vb, near))) + (bias[...],)
+                for own, near in spans
+            ],
+            scale,
+        )
+        for (own, _), (weighted, top, total) in zip(spans, found):
+            acc[:, own, :] = weighted.reshape(res, ROWS_ONE, dim)
+            mx[:, own, :] = top.reshape(res, ROWS_ONE, 1)
+            sm[:, own, :] = total.reshape(res, ROWS_ONE, 1)
 
     def merge(at, weighted, top, total):
         old_top = mx[at].reshape(-1, 1)
@@ -223,35 +250,43 @@
             sm[at].reshape(-1, 1) * old_part + total * part,
         )
 
-    def branch_two(s, b, bias):
-        part = pl.ds(s * RATIO, RATIO)
-        own = pl.ds(b * ROWS_TWO, ROWS_TWO)
-        near = pl.ds(rows + (b - 1) * ROWS_TWO, 2 * ROWS_TWO)
+    def branch_two(blocks, bias):
+        spans = [
+            (
+                pl.ds(s * RATIO, RATIO),
+                pl.ds(b * ROWS_TWO, ROWS_TWO),
+                pl.ds(rows + (b - 1) * ROWS_TWO, 2 * ROWS_TWO),
+            )
+            for s, b in blocks
+        ]
         found = attend(
-            qb[part, own, :].reshape(-1, dim), kb[part, near, :].reshape(-1, dim), vb[part, near, :].reshape(-1, dim),
-            bias[...], scale,
-        )
-        at = (part, own, slice(None))
-        weighted, top, total = merge(at, *found)
-        acc[at] = weighted.reshape(RATIO, ROWS_TWO, dim)
-        mx[at] = top.reshape(RATIO, ROWS_TWO, 1)
-        sm[at] = total.reshape(RATIO, ROWS_TWO, 1)
-
-    for b in range(1, rows // ROWS_ONE):
-        branch_one(b, bias1)
-    for s in range(CHUNKS):
-        for b in range(1, rows // ROWS_TWO):
-            branch_two(s, b, bias2)
+            [
+                tuple(x[part, at, :].reshape(-1, dim) for x, at in ((qb, own), (kb, near), (vb, near))) + (bias[...],)
+                for part, own, near in spans
+            ],
+            scale,
+        )
+        merged = [merge((part, own, slice(None)), *one) for (part, own, _), one in zip(spans, found)]
+        for (part, own, _), (weighted, top, total) in zip(spans, merged):
+            acc[part, own, :] = weighted.reshape(RATIO, ROWS_TWO, dim)
+            mx[part, own, :] = top.reshape(RATIO, ROWS_TWO, 1)
+            sm[part, own, :] = total.reshape(RATIO, ROWS_TWO, 1)
+
+    def some(items, count):
+        return [items[i : i + count] for i in range(0, len(items), count)]
+
+    for blocks in some(list(range(1, rows // ROWS_ONE)), 2):
+        branch_one(blocks, bias1)
+    for blocks in some([(s, b) for s in range(CHUNKS) for b in range(1, rows // ROWS_TWO)], 4):
+        branch_two(blocks, bias2)
 
     @pl.when(has_prev)
     def _():
-        for k in range(group - 1):
+        for k in range(group):
             for which in (0, 1):
-                onward(which, k).wait_recv()
-
-    branch_one(0, bias1f)
-    for s in range(CHUNKS):
-        branch_two(s, 0, bias2f)
+                onward_rows(which, k).wait_recv()
+
+    branch_one([0], bias1f)
 
     head = tp * group + mine
 
@@ -260,31 +295,30 @@
 
     def give(s, d):
         part = pl.ds(s * RATIO, RATIO)
-        other = lax.rem(mine + d, group)
+        other = member(d)
         return pltpu.make_async_remote_copy(
             src_ref=ob.at[part, span(piece * other), :],
             dst_ref=ab.at[part, :, lanes(head)],
             send_sem=o_send.at[s, d],
-            recv_sem=o_recv.at[s, mine],
+            recv_sem=o_recv.at[s, d],
             device_id={"sp": base + other},
             device_id_type=MESH,
         )
 
-    def taken(s, origin):
+    def taken(s, d):
         part = pl.ds(s * RATIO, RATIO)
         return pltpu.make_async_remote_copy(
             src_ref=ob.at[part, span(0), :],
-            dst_ref=ab.at[part, :, lanes(tp * group + origin)],
-            send_sem=o_send.at[s, 0],
-            recv_sem=o_recv.at[s, origin],
+            dst_ref=ab.at[part, :, lanes(tp * group + member(d))],
+            send_sem=o_send.at[s, d],
+            recv_sem=o_recv.at[s, d],
             device_id={"sp": sp},
             device_id_type=MESH,
         )
 
     def swap(s, d):
         part = pl.ds(s * RATIO, RATIO)
-        origin = lax.rem(mine + d, group)
-        slot = ab.at[part, :, lanes(tp * group + origin)]
+        slot = ab.at[part, :, lanes(tp * group + member(d))]
         return pltpu.make_async_remote_copy(
             src_ref=ob.at[part, span(piece * mine), :] if d == 0 else slot,
             dst_ref=slot,
@@ -296,39 +330,21 @@
 
     def swapped(s, d):
         part = pl.ds(s * RATIO, RATIO)
-        origin = lax.rem(mine + d, group)
         return pltpu.make_async_remote_copy(
             src_ref=ob.at[part, span(0), :],
-            dst_ref=ab.at[part, :, lanes(partner * group + origin)],
+            dst_ref=ab.at[part, :, lanes(partner * group + member(d))],
             send_sem=d_send.at[s, d],
             recv_sem=d_recv.at[s, d],
             device_id={"tp": partner},
             device_id_type=MESH,
         )
 
-    for s in range(CHUNKS):
-        part = pl.ds(s * RATIO, RATIO)
-
-        @pl.when(has_prev)
-        def _():
-            for which in (0, 1):
-                onward_last(which, s).wait_recv()
-
-        for store in range(s * RATIO, (s + 1) * RATIO):
-            found = attend(qb[store], kb[store], vb[store], bias3[...], scale)
-            weighted, _, total = merge((store,), *found)
-            ob[store] = (weighted / total).astype(ob.dtype)
+    def hand_over(s):
         for d in range(1, group):
-            give(s, d).start()
-        swap(s, 0).start()
-        ab[part, :, lanes(head)] = ob[part, span(piece * mine), :]
-
-    for s in range(CHUNKS):
-        part = pl.ds(s * RATIO, RATIO)
-        for d in range(1, group):
-            taken(s, lax.rem(mine + d, group)).wait_recv()
+            taken(s, d).wait_recv()
             swap(s, d).start()
-    for s in range(CHUNKS):
+
+    def project(s):
         part = pl.ds(s * RATIO, RATIO)
         for d in range(group):
             swapped(s, d).wait_recv()
@@ -336,6 +352,33 @@
         mixed = jnp.dot(attended, w_ref[...], preferred_element_type=jnp.float32)
         o_ref[part] = mixed.astype(o_ref.dtype).reshape(RATIO, piece, -1)
 
+    for s in range(CHUNKS):
+        part = pl.ds(s * RATIO, RATIO)
+
+        @pl.when(has_prev)
+        def _():
+            for k in split:
+                for which in (0, 1):
+                    onward_chunk(which, k, s).wait_recv()
+
+        branch_two([(s, 0)], bias2f)
+        stores = range(s * RATIO, (s + 1) * RATIO)
+        found = attend([(qb[x], kb[x], vb[x], bias3[...]) for x in stores], scale)
+        for x, one in zip(stores, found):
+            weighted, _, total = merge((x,), *one)
+            ob[x] = (weighted / total).astype(ob.dtype)
+        for d in far + near:
+            give(s, d).start()
+        swap(s, 0).start()
+        ab[part, :, lanes(head)] = ob[part, span(piece * mine), :]
+        if s >= 2:
+            hand_over(s - 2)
+    for s in range(CHUNKS - 2, CHUNKS):
+        hand_over(s)
+        project(s - 2)
+    for s in range(CHUNKS - 2, CHUNKS):
+        project(s)
+
     for which in (0, 1, 2):
         for d in range(1, group):
             exchange(which, d).wait_send()
@@ -343,10 +386,11 @@
     @pl.when(has_next)
     def _():
         for which in (0, 1):
-            for k in range(group - 1):
-                onward(which, k).wait_send()
-            for s in range(CHUNKS):
-                onward_last(which, s).wait_send()
+            for k in range(group):
+                onward_rows(which, k).wait_send()
+            for k in split:
+                for s in range(CHUNKS):
+                    onward_chunk(which, k, s).wait_send()
 
     for s in range(CHUNKS):
         for d in range(1, group):
@@ -361,6 +405,7 @@
     res = DILATION_THREE
     piece = tokens // res
     rows = group * piece
+    assert group & (group - 1) == 0 and piece > ROWS_ONE
     assert group * tokens == WINDOW_THREE and lax.axis_size("sp") % group == 0 and lax.axis_size("tp") == 2
 
     def by_residue(x):
@@ -391,7 +436,7 @@
             pltpu.VMEM((rows, 2 * rows), full),
             dma((3, group)), dma((3, group)),
             dma((2, group)), dma((2, group)),
-            dma((2, CHUNKS)), dma((2, CHUNKS)),
+            dma((2, group, CHUNKS)), dma((2, group, CHUNKS)),
             dma((CHUNKS, group)), dma((CHUNKS, group)),
             dma((CHUNKS, group)), dma((CHUNKS, group)),
         ],

time: 50.1 us -> 47.6 us (0.950)
  the two profiles are of different devices: /device:TPU:19 before, /device:TPU:0 now
where the time goes in v2:
time: 47.6 us; the launch traced here: 47.4 us
  Pallas kernels  41.1 us (86%)
  local copies, waits for them, and re-layouts  6.23 us (13%)
    pallas_call x1, Pallas kernels, local(): pl.pallas_call(functools.partial(kernel, group), out_shape=jax.ShapeDtype...  41.1 us
    reshape x3, local copies, waits for them, and re-layouts, by_residue(): x = x.reshape(piece, RATIO, DILATION_TWO, group, dim)  4.31 us
    reshape x1, local copies, waits for them, and re-layouts, local(): return jnp.transpose(mixed, (2, 1, 0, 3)).reshape(tokens, columns)  1.11 us

profile of v2, /device:TPU:0, one launch (start us, length us, event | category | flops | bytes accessed | tf_op | source)
XLA Modules:
  0.0 47.4 jit_solution(11480743025456289192)
XLA Ops:
  0.0 0.0 copy-start
  0.0 1.5 %copy.5 = bf16[32,4,4,4,128]{4,0,1,2,3:T(8,128)(2,1)S(1)} copy(bf16[32,4,4,4,128]{4,3,2,1,0:T(4,128)(2,1)} %bitcast.19) | data formatting | bytes 1048576 | tf_op jit(solution)/shard_map/reshape | solution.py:412
  1.5 1.4 %copy.6 = bf16[32,4,4,4,128]{4,0,1,2,3:T(8,128)(2,1)S(1)} copy(bf16[32,4,4,4,128]{4,3,2,1,0:T(4,128)(2,1)} %bitcast.20) | data formatting | bytes 1048576 | tf_op jit(solution)/shard_map/reshape | solution.py:412
  2.9 1.4 %copy.7 = bf16[32,4,4,4,128]{4,0,1,2,3:T(8,128)(2,1)S(1)} copy(bf16[32,4,4,4,128]{4,3,2,1,0:T(4,128)(2,1)} %bitcast.21) | data formatting | bytes 1048576 | tf_op jit(solution)/shard_map/reshape | solution.py:412
  4.3 0.0 copy-done
  4.3 41.1 %shard_map.46 = bf16[16,32,1024]{2,1,0:T(8,128)(2,1)S(1)} custom-call(bf16[4,16,32,128]{3,2,1,0:T(8,128)(2,1)S(1)} %bitcast.16, bf16[4,16,32,128]{3,2,1,0:T(8,128)(2,1)S(1)} %bitcast.17, bf16[4,16,32,128]{3,2,1,0:T(8,128)(2,1)S(1)} %bitcast.18, bf16[1024,1024]{1,0:T(8,128)(2,1)S(1)} %copy-done), custom_call_target="tpu_custom_call" | custom-call | tf_op jit(solution)/shard_map/pallas_call | solution.py:418
  45.4 0.8 %copy.8 = bf16[32,4,4,1024]{3,2,1,0:T(4,128)(2,1)S(1)} copy(bf16[32,4,4,1024]{3,0,1,2:T(8,128)(2,1)S(1)} %bitcast.15) | data formatting | bytes 2097152 | tf_op jit(solution)/shard_map/transpose | solution.py:448
  46.3 1.1 %reshape.31 = bf16[512,1024]{1,0:T(8,128)(2,1)} reshape(bf16[32,4,4,1024]{3,2,1,0:T(4,128)(2,1)S(1)} %copy.8) | data formatting | bytes 2097152 | tf_op jit(solution)/shard_map/reshape | solution.py:448
Async XLA Ops:
  0.0 4.3 %copy-start = (bf16[1024,1024]{1,0:T(8,128)(2,1)S(1)}, bf16[1024,1024]{1,0:T(8,128)(2,1)}, u32[]{:S(2)}) copy-start(bf16[1024,1024]{1,0:T(8,128)(2,1)} %w_ref.1) | copy-start | bytes 6291460

commit v3 on v2

--- a/solution.py
+++ b/solution.py
@@ -28,12 +28,14 @@
     scores = [x * scale + bias for x, (_, _, _, bias) in zip(scores, blocks)]
     tops = [jnp.max(x, axis=-1, keepdims=True) for x in scores]
     numerators = [jnp.exp2(x - top) for x, top in zip(scores, tops)]
-    totals = [jnp.sum(x, axis=-1, keepdims=True) for x in numerators]
-    weighted = [
-        jnp.dot(x.astype(jnp.bfloat16), v, preferred_element_type=jnp.float32)
+    sums = [
+        jnp.dot(
+            x.astype(v.dtype), jnp.concatenate([v, jnp.ones_like(v)], axis=1), preferred_element_type=jnp.float32
+        )
         for x, (_, _, v, _) in zip(numerators, blocks)
     ]
-    return list(zip(weighted, tops, totals))
+    dim = blocks[0][2].shape[-1]
+    return [(x[:, :dim], jnp.broadcast_to(top, x[:, :dim].shape), x[:, dim:]) for x, top in zip(sums, tops)]
 
 
 def bias_of(shape, place_q, place_k, first_own, window, has_prev):
@@ -237,17 +239,17 @@
         )
         for (own, _), (weighted, top, total) in zip(spans, found):
             acc[:, own, :] = weighted.reshape(res, ROWS_ONE, dim)
-            mx[:, own, :] = top.reshape(res, ROWS_ONE, 1)
-            sm[:, own, :] = total.reshape(res, ROWS_ONE, 1)
+            mx[:, own, :] = top.reshape(res, ROWS_ONE, dim)
+            sm[:, own, :] = total.reshape(res, ROWS_ONE, dim)
 
     def merge(at, weighted, top, total):
-        old_top = mx[at].reshape(-1, 1)
+        old_top = mx[at].reshape(-1, dim)
         new_top = jnp.maximum(old_top, top)
         old_part, part = jnp.exp2(old_top - new_top), jnp.exp2(top - new_top)
         return (
             acc[at].reshape(-1, dim) * old_part + weighted * part,
             new_top,
-            sm[at].reshape(-1, 1) * old_part + total * part,
+            sm[at].reshape(-1, dim) * old_part + total * part,
         )
 
     def branch_two(blocks, bias):
@@ -269,15 +271,15 @@
         merged = [merge((part, own, slice(None)), *one) for (part, own, _), one in zip(spans, found)]
         for (part, own, _), (weighted, top, total) in zip(spans, merged):
             acc[part, own, :] = weighted.reshape(RATIO, ROWS_TWO, dim)
-            mx[part, own, :] = top.reshape(RATIO, ROWS_TWO, 1)
-            sm[part, own, :] = total.reshape(RATIO, ROWS_TWO, 1)
+            mx[part, own, :] = top.reshape(RATIO, ROWS_TWO, dim)
+            sm[part, own, :] = total.reshape(RATIO, ROWS_TWO, dim)
 
     def some(items, count):
         return [items[i : i + count] for i in range(0, len(items), count)]
 
-    for blocks in some(list(range(1, rows // ROWS_ONE)), 2):
+    for blocks in some(list(range(1, rows // ROWS_ONE)), 1):
         branch_one(blocks, bias1)
-    for blocks in some([(s, b) for s in range(CHUNKS) for b in range(1, rows // ROWS_TWO)], 4):
+    for blocks in some([(s, b) for s in range(CHUNKS) for b in range(1, rows // ROWS_TWO)], 2):
         branch_two(blocks, bias2)
 
     @pl.when(has_prev)
@@ -362,11 +364,11 @@
                     onward_chunk(which, k, s).wait_recv()
 
         branch_two([(s, 0)], bias2f)
-        stores = range(s * RATIO, (s + 1) * RATIO)
-        found = attend([(qb[x], kb[x], vb[x], bias3[...]) for x in stores], scale)
-        for x, one in zip(stores, found):
-            weighted, _, total = merge((x,), *one)
-            ob[x] = (weighted / total).astype(ob.dtype)
+        for stores in some(list(range(s * RATIO, (s + 1) * RATIO)), 2):
+            found = attend([(qb[x], kb[x], vb[x], bias3[...]) for x in stores], scale)
+            for x, one in zip(stores, found):
+                weighted, _, total = merge((x,), *one)
+                ob[x] = (weighted / total).astype(ob.dtype)
         for d in far + near:
             give(s, d).start()
         swap(s, 0).start()
@@ -425,8 +427,8 @@
             pltpu.VMEM((res, 2 * rows, dim), low),
             pltpu.VMEM((res, 2 * rows, dim), low),
             pltpu.VMEM((res, rows, dim), full),
-            pltpu.VMEM((res, rows, 1), full),
-            pltpu.VMEM((res, rows, 1), full),
+            pltpu.VMEM((res, rows, dim), full),
+            pltpu.VMEM((res, rows, dim), full),
             pltpu.VMEM((res, rows, dim), low),
             pltpu.VMEM((res, piece, features), low),
             pltpu.VMEM((res * ROWS_ONE, 2 * res * ROWS_ONE), full),

time: 47.6 us -> 44.6 us (0.937)
  Pallas kernels: 41.1 us -> 38.1 us
    pallas_call x1, Pallas kernels: 41.1 us -> 38.1 us  [local(): pl.pallas_call(functools.partial(kernel, group), out_shape=jax.ShapeDtype...]
where the time goes in v3:
time: 44.6 us; the launch traced here: 44.4 us
  Pallas kernels  38.1 us (85%)
  local copies, waits for them, and re-layouts  6.23 us (14%)
    pallas_call x1, Pallas kernels, local(): pl.pallas_call(functools.partial(kernel, group), out_shape=jax.ShapeDtype...  38.1 us
    reshape x3, local copies, waits for them, and re-layouts, by_residue(): x = x.reshape(piece, RATIO, DILATION_TWO, group, dim)  4.31 us
    reshape x1, local copies, waits for them, and re-layouts, local(): return jnp.transpose(mixed, (2, 1, 0, 3)).reshape(tokens, columns)  1.11 us

profile of v3, /device:TPU:0, one launch (start us, length us, event | category | flops | bytes accessed | tf_op | source)
XLA Modules:
  0.0 44.4 jit_solution(6484987149541333117)
XLA Ops:
  0.0 0.0 copy-start
  0.0 1.5 %copy.5 = bf16[32,4,4,4,128]{4,0,1,2,3:T(8,128)(2,1)S(1)} copy(bf16[32,4,4,4,128]{4,3,2,1,0:T(4,128)(2,1)} %bitcast.19) | data formatting | bytes 1048576 | tf_op jit(solution)/shard_map/reshape | solution.py:414
  1.5 1.4 %copy.6 = bf16[32,4,4,4,128]{4,0,1,2,3:T(8,128)(2,1)S(1)} copy(bf16[32,4,4,4,128]{4,3,2,1,0:T(4,128)(2,1)} %bitcast.20) | data formatting | bytes 1048576 | tf_op jit(solution)/shard_map/reshape | solution.py:414
  2.9 1.4 %copy.7 = bf16[32,4,4,4,128]{4,0,1,2,3:T(8,128)(2,1)S(1)} copy(bf16[32,4,4,4,128]{4,3,2,1,0:T(4,128)(2,1)} %bitcast.21) | data formatting | bytes 1048576 | tf_op jit(solution)/shard_map/reshape | solution.py:414
  4.3 0.0 copy-done
  4.3 38.1 %shard_map.46 = bf16[16,32,1024]{2,1,0:T(8,128)(2,1)S(1)} custom-call(bf16[4,16,32,128]{3,2,1,0:T(8,128)(2,1)S(1)} %bitcast.16, bf16[4,16,32,128]{3,2,1,0:T(8,128)(2,1)S(1)} %bitcast.17, bf16[4,16,32,128]{3,2,1,0:T(8,128)(2,1)S(1)} %bitcast.18, bf16[1024,1024]{1,0:T(8,128)(2,1)S(1)} %copy-done), custom_call_target="tpu_custom_call" | custom-call | tf_op jit(solution)/shard_map/pallas_call | solution.py:420
  42.4 0.8 %copy.8 = bf16[32,4,4,1024]{3,2,1,0:T(4,128)(2,1)S(1)} copy(bf16[32,4,4,1024]{3,0,1,2:T(8,128)(2,1)S(1)} %bitcast.15) | data formatting | bytes 2097152 | tf_op jit(solution)/shard_map/transpose | solution.py:450
  43.3 1.1 %reshape.31 = bf16[512,1024]{1,0:T(8,128)(2,1)} reshape(bf16[32,4,4,1024]{3,2,1,0:T(4,128)(2,1)S(1)} %copy.8) | data formatting | bytes 2097152 | tf_op jit(solution)/shard_map/reshape | solution.py:450
Async XLA Ops:
  0.0 4.3 %copy-start = (bf16[1024,1024]{1,0:T(8,128)(2,1)S(1)}, bf16[1024,1024]{1,0:T(8,128)(2,1)}, u32[]{:S(2)}) copy-start(bf16[1024,1024]{1,0:T(8,128)(2,1)} %w_ref.1) | copy-start | bytes 6291460

commit v4 on v3

--- a/solution.py
+++ b/solution.py
@@ -223,12 +223,13 @@
                 for which in (0, 1):
                     onward_chunk(which, k, s).start()
 
-    for k in range(1, group):
-        arrival(2, k).wait_recv()
-
     def branch_one(blocks, bias):
         spans = [
-            (pl.ds(b * ROWS_ONE, ROWS_ONE), pl.ds(rows + (b - 1) * ROWS_ONE, 2 * ROWS_ONE)) for b in blocks
+            (
+                pl.ds(pl.multiple_of(b * ROWS_ONE, ROWS_ONE), ROWS_ONE),
+                pl.ds(pl.multiple_of(rows + (b - 1) * ROWS_ONE, ROWS_ONE), 2 * ROWS_ONE),
+            )
+            for b in blocks
         ]
         found = attend(
             [
@@ -277,8 +278,14 @@
     def some(items, count):
         return [items[i : i + count] for i in range(0, len(items), count)]
 
-    for blocks in some(list(range(1, rows // ROWS_ONE)), 1):
-        branch_one(blocks, bias1)
+    steps = piece // ROWS_ONE
+    for d in [0] + near + far:
+        if d:
+            arrival(2, d).wait_recv()
+        for inner in range(1, steps):
+            branch_one([member(d) * steps + inner], bias1)
+    for b in range(steps, rows // ROWS_ONE, steps):
+        branch_one([b], bias1)
     for blocks in some([(s, b) for s in range(CHUNKS) for b in range(1, rows // ROWS_TWO)], 2):
         branch_two(blocks, bias2)
 

time: 44.6 us -> 44.2 us (level)
  no operation moved by 1% of the time
where the time goes in v4:
time: 44.2 us; the launch traced here: 44 us
  Pallas kernels  37.7 us (85%)
  local copies, waits for them, and re-layouts  6.23 us (14%)
    pallas_call x1, Pallas kernels, local(): pl.pallas_call(functools.partial(kernel, group), out_shape=jax.ShapeDtype...  37.7 us
    reshape x3, local copies, waits for them, and re-layouts, by_residue(): x = x.reshape(piece, RATIO, DILATION_TWO, group, dim)  4.31 us
    reshape x1, local copies, waits for them, and re-layouts, local(): return jnp.transpose(mixed, (2, 1, 0, 3)).reshape(tokens, columns)  1.11 us

profile of v4, /device:TPU:0, one launch (start us, length us, event | category | flops | bytes accessed | tf_op | source)
XLA Modules:
  0.0 44.0 jit_solution(1735908423102288559)
XLA Ops:
  0.0 0.0 copy-start
  0.0 1.5 %copy.5 = bf16[32,4,4,4,128]{4,0,1,2,3:T(8,128)(2,1)S(1)} copy(bf16[32,4,4,4,128]{4,3,2,1,0:T(4,128)(2,1)} %bitcast.19) | data formatting | bytes 1048576 | tf_op jit(solution)/shard_map/reshape | solution.py:421
  1.5 1.4 %copy.6 = bf16[32,4,4,4,128]{4,0,1,2,3:T(8,128)(2,1)S(1)} copy(bf16[32,4,4,4,128]{4,3,2,1,0:T(4,128)(2,1)} %bitcast.20) | data formatting | bytes 1048576 | tf_op jit(solution)/shard_map/reshape | solution.py:421
  2.9 1.4 %copy.7 = bf16[32,4,4,4,128]{4,0,1,2,3:T(8,128)(2,1)S(1)} copy(bf16[32,4,4,4,128]{4,3,2,1,0:T(4,128)(2,1)} %bitcast.21) | data formatting | bytes 1048576 | tf_op jit(solution)/shard_map/reshape | solution.py:421
  4.3 0.0 copy-done
  4.3 37.7 %shard_map.46 = bf16[16,32,1024]{2,1,0:T(8,128)(2,1)S(1)} custom-call(bf16[4,16,32,128]{3,2,1,0:T(8,128)(2,1)S(1)} %bitcast.16, bf16[4,16,32,128]{3,2,1,0:T(8,128)(2,1)S(1)} %bitcast.17, bf16[4,16,32,128]{3,2,1,0:T(8,128)(2,1)S(1)} %bitcast.18, bf16[1024,1024]{1,0:T(8,128)(2,1)S(1)} %copy-done), custom_call_target="tpu_custom_call" | custom-call | tf_op jit(solution)/shard_map/pallas_call | solution.py:427
  42.1 0.8 %copy.8 = bf16[32,4,4,1024]{3,2,1,0:T(4,128)(2,1)S(1)} copy(bf16[32,4,4,1024]{3,0,1,2:T(8,128)(2,1)S(1)} %bitcast.15) | data formatting | bytes 2097152 | tf_op jit(solution)/shard_map/transpose | solution.py:457
  42.9 1.1 %reshape.31 = bf16[512,1024]{1,0:T(8,128)(2,1)} reshape(bf16[32,4,4,1024]{3,2,1,0:T(4,128)(2,1)S(1)} %copy.8) | data formatting | bytes 2097152 | tf_op jit(solution)/shard_map/reshape | solution.py:457
Async XLA Ops:
  0.0 4.3 %copy-start = (bf16[1024,1024]{1,0:T(8,128)(2,1)S(1)}, bf16[1024,1024]{1,0:T(8,128)(2,1)}, u32[]{:S(2)}) copy-start(bf16[1024,1024]{1,0:T(8,128)(2,1)} %w_ref.1) | copy-start | bytes 6291460
